TPU v7x, 32 devices: a whole 2x2x4 slice. The times are simulated.
32 devices in a mesh: sp: 4 (over z), fs: 4 (over y, x), tp: 2 (over core).
Axes of the slice: x: 2, y: 2, z: 4, core: 2. Of those that a mesh axis runs over, the one named last changes fastest.
Arguments:
- tokens: bfloat16 [4, 512, 2048], P('fs', ('sp', 'tp')), may hold values from -6 to 6
- norm_gain: float32 [2048], replicated, may hold values from 0.1 to 1.9
- gla_query_weight: bfloat16 [2048, 512], P('sp', 'tp'), may hold values from -0.125 to 0.125
- gla_key_weight: bfloat16 [2048, 512], P('sp', 'tp'), may hold values from -0.125 to 0.125
- gla_value_weight: bfloat16 [2048, 1024], P('sp', 'tp'), may hold values from -0.125 to 0.125
- decay_down: bfloat16 [2048, 32], P('sp'), may hold values from -0.125 to 0.125
- decay_up: bfloat16 [32, 512], P(None, 'tp'), may hold values from -1 to 1
- decay_bias: float32 [512], P('tp'), may hold values from 0.5 to 12
- head_gain: float32 [128], replicated, may hold values from 0.1 to 1.9
- window_query_weight: bfloat16 [2048, 1024], P('sp', 'tp'), may hold values from -3 to 3
- window_key_weight: bfloat16 [2048, 256], P('sp', 'tp'), may hold values from -3 to 3
- window_value_weight: bfloat16 [2048, 256], P('sp', 'tp'), may hold values from -0.125 to 0.125
- sink_logit: float32 [16], P('tp'), may hold values from 3 to 7
- gla_output_weight: bfloat16 [1024, 2048], P('tp', 'sp'), may hold values from -0.125 to 0.125
- window_output_weight: bfloat16 [1024, 2048], P('tp', 'sp'), may hold values from -0.125 to 0.125
Outputs:
- mixed: bfloat16 [4, 512, 2048], P('fs', ('sp', 'tp'))
All inputs are finite; a program needn't handle non-finite values.
Results may differ from a plain program's by a relative error of at most 0.013.
Values may be sent and summed in bfloat16 or wider, within the bound.
A program may use at most 64 MiB of HBM per device.

v0:
```python
import jax
import jax.numpy as jnp
from jax import lax
from jax.sharding import PartitionSpec as P

KEY_DIM = 64
VALUE_DIM = 128
SWA_HEADS = 16
KV_HEADS = 4
HEAD_DIM = 64
WINDOW = 128
SPAN = 64


EPS = 1e-06
SOFTMAX_TEMPER = 16.0
HIGH = lax.Precision.HIGHEST


def entering_2(value, axis, join, neutral):
    count, mine = (lax.axis_size(axis), lax.axis_index(axis))
    pieces = jax.tree.map(lambda part: lax.all_gather(part, axis), value)
    subtotal = jax.tree.map(
        lambda part, zero: jnp.full_like(part, 0) + jnp.asarray(zero, part.dtype), value, neutral
    )

    def step(position, subtotal):
        longer = join(subtotal, jax.tree.map(lambda part: part[position], pieces))
        return jax.tree.map(lambda new, old: jnp.where(position < mine, new, old), longer, subtotal)

    return lax.fori_loop(0, count - 1, step, subtotal)


def passed_along(value, axis, by):
    peers = lax.axis_size(axis)
    pairs = [(i, i + by) for i in range(peers) if 0 <= i + by < peers]
    return lax.ppermute(value, axis, pairs)


def rms_rows(values, gain):
    mean_square = jnp.mean(values * values, axis=-1, keepdims=True)
    return values * lax.rsqrt(mean_square + EPS) * gain


def block_terms(query_rows, key_rows, value_rows, log_decay_rate, block_len):
    seq_len, head_count, key_width = query_rows.shape
    value_width = value_rows.shape[-1]
    block_count = seq_len // block_len
    q_scaled = query_rows.reshape(block_count, block_len, head_count, key_width) * key_width ** (
        -0.5
    )
    k_blocks = key_rows.reshape(block_count, block_len, head_count, key_width)
    v_blocks = value_rows.reshape(block_count, block_len, head_count, value_width)
    within = jnp.cumsum(
        log_decay_rate.reshape(block_count, block_len, head_count, key_width), axis=1
    )
    block_total = within[:, -1]
    q_dec = q_scaled * jnp.exp(within)
    k_dec = k_blocks * jnp.exp(-within)
    k_end = k_blocks * jnp.exp(block_total[:, None] - within)
    causal = jnp.tril(jnp.ones((block_len, block_len), dtype=bool))
    scores = jnp.einsum("nihd,njhd->nhij", q_dec, k_dec, precision=HIGH)
    scores = jnp.where(causal, scores, 0.0)
    local_out = jnp.einsum("nhij,njhe->nihe", scores, v_blocks, precision=HIGH)
    update = jnp.einsum("njhd,njhe->nhde", k_end, v_blocks, precision=HIGH)

    def advance(carried, inputs):
        update_in, decay_in = inputs
        return (decay_in[..., None] * carried + update_in, carried)

    start_state = jnp.zeros((head_count, key_width, value_width), jnp.float32)
    last_state, entering = lax.scan(advance, start_state, (update, jnp.exp(block_total)))
    return (q_dec, local_out, entering, last_state, block_total)


def window_band_mask(block_count, block_len, offset):
    query_pos = jnp.arange(block_len)[:, None] + block_len
    key_pos = jnp.arange(2 * block_len)[None, :]
    distance = query_pos - key_pos
    inside = (distance >= 0) & (distance < block_len)
    global_key = (
        offset + jnp.arange(block_count)[:, None, None] * block_len - block_len + key_pos[None]
    )
    return inside[None] & (global_key >= 0)


def window_attend(query_blocks, key_band, value_band, valid, sinks):
    scores = jnp.einsum(
        "nqhgd,nkhd->nhgqk", query_blocks, key_band, preferred_element_type=jnp.float32
    )
    scores = scores * HEAD_DIM ** (-0.5)
    scores = jnp.where(valid[:, None, None], scores, -1e30)
    sink_term = sinks[None, :, :, None, None]
    top = jnp.maximum(jnp.max(scores, axis=-1, keepdims=True), sink_term)
    expo = jnp.exp(scores - top)
    denom = jnp.sum(expo, axis=-1, keepdims=True) + jnp.exp(sink_term - top)
    weights = (expo / denom).astype(jnp.bfloat16)
    attended = jnp.einsum(
        "nhgqk,nkhd->nqhgd", weights, value_band, preferred_element_type=jnp.float32
    )
    return attended.astype(jnp.bfloat16)


def quarter(weight, along):
    piece_width = weight.shape[along] // lax.axis_size("fs")
    return lax.dynamic_slice_in_dim(weight, lax.axis_index("fs") * piece_width, piece_width, along)


def per_device(
    tokens,
    norm_gain,
    gla_query_weight,
    gla_key_weight,
    gla_value_weight,
    decay_down,
    decay_up,
    decay_bias,
    head_gain,
    window_query_weight,
    window_key_weight,
    window_value_weight,
    sink_logit,
    gla_output_weight,
    window_output_weight,
):
    seq_rows = lax.all_gather(tokens, "tp", axis=1, tiled=True)[0]
    tok_rows = seq_rows.shape[0]
    pieces = (
        lax.all_gather(quarter(gla_query_weight, 1), "sp", axis=0, tiled=True),
        lax.all_gather(quarter(gla_key_weight, 1), "sp", axis=0, tiled=True),
        lax.all_gather(quarter(gla_value_weight, 1), "sp", axis=0, tiled=True),
        lax.all_gather(quarter(decay_down, 1), "sp", axis=0, tiled=True),
        lax.all_gather(quarter(window_query_weight, 1), "sp", axis=0, tiled=True),
        lax.all_gather(quarter(window_key_weight, 1), "sp", axis=0, tiled=True),
        lax.all_gather(quarter(window_value_weight, 1), "sp", axis=0, tiled=True),
    )
    input_maps = (
        lax.all_gather(pieces[0], "fs", axis=1, tiled=True),
        lax.all_gather(pieces[1], "fs", axis=1, tiled=True),
        lax.all_gather(pieces[2], "fs", axis=1, tiled=True),
        lax.all_gather(pieces[3], "fs", axis=1, tiled=True),
        lax.all_gather(pieces[4], "fs", axis=1, tiled=True),
        lax.all_gather(pieces[5], "fs", axis=1, tiled=True),
        lax.all_gather(pieces[6], "fs", axis=1, tiled=True),
    )
    out_pieces = (
        lax.all_gather(quarter(gla_output_weight, 0), "sp", axis=1, tiled=True),
        lax.all_gather(quarter(window_output_weight, 0), "sp", axis=1, tiled=True),
    )
    output_maps = (
        lax.all_gather(out_pieces[0], "fs", axis=0, tiled=True),
        lax.all_gather(out_pieces[1], "fs", axis=0, tiled=True),
    )
    normed = rms_rows(seq_rows.astype(jnp.float32), norm_gain).astype(jnp.bfloat16)

    def project(weight):
        return jnp.dot(normed, weight, preferred_element_type=jnp.float32).astype(jnp.bfloat16)

    seq_offset = lax.axis_index("sp") * tok_rows
    window_query = project(input_maps[4])
    sliding_key = project(input_maps[5])
    window_value = project(input_maps[6])
    kv_local = sliding_key.shape[1] // HEAD_DIM
    group_size = SWA_HEADS // KV_HEADS
    block_count = tok_rows // WINDOW
    edge_keys, edge_values = passed_along((sliding_key, window_value), "sp", 1)

    def banded(rows, edge_rows):
        blocks = rows.reshape(block_count, WINDOW, kv_local, HEAD_DIM)
        edge_block = edge_rows.reshape(1, WINDOW, kv_local, HEAD_DIM)
        earlier = jnp.concatenate([edge_block, blocks[:-1]], axis=0)
        return jnp.concatenate([earlier, blocks], axis=1)

    query_blocks = window_query.reshape(block_count, WINDOW, kv_local, group_size, HEAD_DIM)
    valid = window_band_mask(block_count, WINDOW, seq_offset)
    sinks = sink_logit.reshape(kv_local, group_size)
    attended = window_attend(
        query_blocks,
        banded(sliding_key, edge_keys),
        banded(window_value, edge_values),
        valid,
        sinks,
    )
    window_hidden = attended.reshape(tok_rows, kv_local * group_size * HEAD_DIM)
    gla_query = project(input_maps[0])
    gla_key = project(input_maps[1])
    gla_value = project(input_maps[2])
    low_rank = project(input_maps[3])
    gate_logit_values = jnp.dot(low_rank, decay_up, preferred_element_type=jnp.float32) + decay_bias
    log_decay_rate = jax.nn.log_sigmoid(gate_logit_values) / SOFTMAX_TEMPER
    local_heads = gla_query.shape[1] // KEY_DIM
    q_dec, local_out, entering, last_state, block_total = block_terms(
        gla_query.astype(jnp.float32).reshape(tok_rows, local_heads, KEY_DIM),
        gla_key.astype(jnp.float32).reshape(tok_rows, local_heads, KEY_DIM),
        gla_value.astype(jnp.float32).reshape(tok_rows, local_heads, VALUE_DIM),
        log_decay_rate.reshape(tok_rows, local_heads, KEY_DIM),
        SPAN,
    )
    device_decay = jnp.exp(jnp.sum(block_total, axis=0))

    def combine(earlier, later):
        return (later[1][..., None] * earlier[0] + later[0], earlier[1] * later[1])

    identity = (jnp.zeros_like(last_state), jnp.ones_like(device_decay))
    incoming = entering_2((last_state, device_decay), "sp", combine, identity)[0]
    before = jnp.cumsum(block_total, axis=0) - block_total
    entering_all = entering + jnp.exp(before)[..., None] * incoming[None]
    gla_out = local_out + jnp.einsum("nihd,nhde->nihe", q_dec, entering_all, precision=HIGH)
    gla_out = gla_out.reshape(tok_rows, local_heads, VALUE_DIM)
    gla_hidden = (
        rms_rows(gla_out, head_gain).astype(jnp.bfloat16).reshape(tok_rows, local_heads * VALUE_DIM)
    )
    own_rows = tok_rows // lax.axis_size("tp")
    total = jnp.dot(gla_hidden, output_maps[0], preferred_element_type=jnp.float32)
    mixed = lax.psum_scatter(
        total + jnp.dot(window_hidden, output_maps[1], preferred_element_type=jnp.float32),
        "tp",
        scatter_dimension=0,
        tiled=True,
    )
    return mixed.astype(jnp.bfloat16).reshape(1, own_rows, mixed.shape[1])


def solution(mesh):
    in_specs = (
        P("fs", ("sp", "tp"), None),
        P(),
        P("sp", "tp"),
        P("sp", "tp"),
        P("sp", "tp"),
        P("sp", None),
        P(None, "tp"),
        P("tp"),
        P(),
        P("sp", "tp"),
        P("sp", "tp"),
        P("sp", "tp"),
        P("tp"),
        P("tp", "sp"),
        P("tp", "sp"),
    )
    out_specs = P("fs", ("sp", "tp"), None)
    return jax.shard_map(
        per_device, mesh=mesh, in_specs=in_specs, out_specs=out_specs, check_vma=False
    )
```

profile of v0, /device:TPU:25, one launch (start us, length us, event | category | flops | bytes accessed | tf_op | source)
XLA Modules:
  0.0 257.1 jit_solution(5551317788708183614)
XLA Ops:
  6.5 1.1 constant_dynamic-slice_fusion.7
  7.7 11.8 %all_gather.70 = bf16[2048,64]{0,1:T(8,128)(2,1)} all-gather(bf16[512,64]{0,1:T(8,128)(2,1)S(1)} %copy.62), channel_id=1, replica_groups=mesh['sp'=4,'fs'=4,'tp'=2] {'sp'}, dimensions={0}, use_global_device_ids=true | all-gather | bytes 327680 | tf_op jit(solution)/shard_map/all_gather | solution.py:129
  19.5 1.0 constant_dynamic-slice_fusion.5
  20.7 13.0 %all_gather.74 = bf16[2048,64]{0,1:T(8,128)(2,1)} all-gather(bf16[512,64]{0,1:T(8,128)(2,1)S(1)} %copy.63), channel_id=1, replica_groups=mesh['sp'=4,'fs'=4,'tp'=2] {'sp'}, dimensions={0}, use_global_device_ids=true | all-gather | bytes 327680 | tf_op jit(solution)/shard_map/all_gather | solution.py:130
  33.8 14.5 %all_gather.68 = bf16[2048,128]{1,0:T(8,128)(2,1)} all-gather(bf16[512,128]{1,0:T(8,128)(2,1)S(1)} %constant_dynamic-slice_fusion.8), channel_id=1, replica_groups=mesh['sp'=4,'fs'=4,'tp'=2] {'sp'}, dimensions={0}, use_global_device_ids=true | all-gather | bytes 655360 | tf_op jit(solution)/shard_map/all_gather | solution.py:131
  48.5 1.0 constant_dynamic-slice_fusion.1
  49.4 14.0 %all_gather.85 = bf16[2048,128]{1,0:T(8,128)(2,1)} all-gather(bf16[512,128]{1,0:T(8,128)(2,1)S(1)} %constant_dynamic-slice_fusion.1), channel_id=1, replica_groups=mesh['sp'=4,'fs'=4,'tp'=2] {'sp'}, dimensions={0}, use_global_device_ids=true | all-gather | bytes 655360 | tf_op jit(solution)/shard_map/all_gather | solution.py:133
  63.5 0.9 constant_dynamic-slice_fusion.4
  64.5 12.8 %all_gather.79 = bf16[128,2048]{1,0:T(8,128)(2,1)} all-gather(bf16[128,512]{1,0:T(8,128)(2,1)S(1)} %constant_dynamic-slice_fusion.4), channel_id=1, replica_groups=mesh['sp'=4,'fs'=4,'tp'=2] {'sp'}, dimensions={1}, use_global_device_ids=true | all-gather | bytes 655360 | tf_op jit(solution)/shard_map/all_gather | solution.py:147
  77.5 11.6 %all_gather.83 = bf16[2048,32]{0,1:T(8,128)(2,1)S(1)} all-gather(bf16[512,32]{0,1:T(8,128)(2,1)S(1)} %copy.65), channel_id=1, replica_groups=mesh['sp'=4,'fs'=4,'tp'=2] {'sp'}, dimensions={0}, use_global_device_ids=true | all-gather | bytes 163840 | tf_op jit(solution)/shard_map/all_gather | solution.py:134
  89.1 10.3 %all_gather.84 = bf16[2048,128]{0,1:T(8,128)(2,1)S(1)} all-gather(bf16[2048,32]{0,1:T(8,128)(2,1)S(1)} %all_gather.83), channel_id=1, replica_groups=mesh['sp'=4,'fs'=4,'tp'=2] {'fs'}, dimensions={1}, use_global_device_ids=true | all-gather | bytes 655360 | tf_op jit(solution)/shard_map/all_gather | solution.py:143
  99.4 21.5 %all_gather.67 = bf16[1,128,2048]{2,1,0:T(8,128)(2,1)S(1)} all-gather(bf16[1,64,2048]{2,1,0:T(8,128)(2,1)S(1)} %copy-done.1), channel_id=1, replica_groups=mesh['sp'=4,'fs'=4,'tp'=2] {'tp'}, dimensions={1}, use_global_device_ids=true | all-gather | bytes 786432 | tf_op jit(solution)/shard_map/all_gather | solution.py:126
  121.5 1.3 collective-permute-start.1
  123.1 10.6 %all_gather.81 = bf16[2048,32]{0,1:T(8,128)(2,1)S(1)} all-gather(bf16[512,32]{0,1:T(8,128)(2,1)S(1)} %copy.64), channel_id=1, replica_groups=mesh['sp'=4,'fs'=4,'tp'=2] {'sp'}, dimensions={0}, use_global_device_ids=true | all-gather | bytes 163840 | tf_op jit(solution)/shard_map/all_gather | solution.py:135
  133.7 8.8 %all_gather.82 = bf16[2048,128]{0,1:T(8,128)(2,1)S(1)} all-gather(bf16[2048,32]{0,1:T(8,128)(2,1)S(1)} %all_gather.81), channel_id=1, replica_groups=mesh['sp'=4,'fs'=4,'tp'=2] {'fs'}, dimensions={1}, use_global_device_ids=true | all-gather | bytes 655360 | tf_op jit(solution)/shard_map/all_gather | solution.py:144
  142.5 1.0 convolution_convert_fusion.6
  143.5 1.4 collective-permute-start
  145.8 13.2 %all_gather.87 = bf16[128,2048]{1,0:T(8,128)(2,1)} all-gather(bf16[128,512]{1,0:T(8,128)(2,1)S(1)} %constant_dynamic-slice_fusion), channel_id=1, replica_groups=mesh['sp'=4,'fs'=4,'tp'=2] {'sp'}, dimensions={1}, use_global_device_ids=true | all-gather | bytes 655360 | tf_op jit(solution)/shard_map/all_gather | solution.py:148
  159.8 10.2 %all_gather.72 = bf16[2048,8]{0,1:T(8,128)(2,1)S(1)} all-gather(bf16[512,8]{0,1:T(8,128)(2,1)S(1)} %constant_dynamic-slice_fusion.6), channel_id=1, replica_groups=mesh['sp'=4,'fs'=4,'tp'=2] {'sp'}, dimensions={0}, use_global_device_ids=true | all-gather | bytes 40960 | tf_op jit(solution)/shard_map/all_gather | solution.py:132
  170.1 6.1 %all_gather.73 = bf16[2048,32]{0,1:T(8,128)(2,1)S(1)} all-gather(bf16[2048,8]{0,1:T(8,128)(2,1)S(1)} %all_gather.72), channel_id=1, replica_groups=mesh['sp'=4,'fs'=4,'tp'=2] {'fs'}, dimensions={1}, use_global_device_ids=true | all-gather | bytes 163840 | tf_op jit(solution)/shard_map/all_gather | solution.py:141
  177.3 8.7 %all-gather.2 = f32[4,4,64]{2,1,0:T(4,128)S(1)} all-gather(f32[1,4,64]{2,1,0:T(4,128)S(1)} %exponential_bitcast_fusion), channel_id=2, replica_groups=mesh['sp'=4,'fs'=4,'tp'=2] {'sp'}, dimensions={0}, use_global_device_ids=true | all-gather | bytes 5120 | tf_op jit(solution)/shard_map/all_gather | solution.py:22
  186.8 1.7 fusion.7
  188.7 1.7 fusion.5
  191.4 2.1 convolution_convert_fusion.2
  194.3 2.2 convolution_convert_fusion.1
  197.2 12.3 %all-gather.1 = f32[16,64,128]{2,1,0:T(8,128)S(1)} all-gather(f32[4,64,128]{2,1,0:T(8,128)S(1)} %get-tuple-element.128), channel_id=3, replica_groups=mesh['sp'=4,'fs'=4,'tp'=2] {'sp'}, dimensions={0}, use_global_device_ids=true | all-gather | bytes 655360 | tf_op jit(solution)/shard_map/all_gather | solution.py:22
  212.0 1.1 convolution_convert_fusion
  213.3 2.0 fusion.23
  215.4 15.3 %all-gather.20.cloned.1.call-done = bf16[512,2048]{1,0:T(8,128)(2,1)} async-done(((bf16[128,2048]{1,0:T(8,128)(2,1)}), bf16[512,2048]{1,0:T(8,128)(2,1)}) %all-gather.20.cloned.1.call-update) | async-done | bytes 2097168 | tf_op jit(solution)/shard_map/all_gather | solution.py:152
  230.7 3.0 %convolution_add_fusion = f32[128,2048]{1,0:T(8,128)} fusion(f32[128,2048]{1,0:T(8,128)S(1)} %fusion.23, bf16[128,512]{0,1:T(8,128)(2,1)S(1)} %bitcast.114, bf16[512,2048]{1,0:T(8,128)(2,1)} %all-gather.20.cloned.1.call-done), kind=kOutput, calls=%fused_computation.6 | convolution fusion | flops 268697600 | bytes 4325376 | tf_op jit(solution)/shard_map/dot_general | solution.py:216
  233.8 14.7 %reduce-scatter.2.cloned.1.call-done = f32[64,2048]{1,0:T(8,128)} async-done(((f32[128,2048]{1,0:T(8,128)}), f32[64,2048]{1,0:T(8,128)}) %reduce-scatter.2.cloned.1.call-update) | async-done | bytes 524304 | tf_op jit(solution)/shard_map/reduce_scatter | solution.py:215
  248.5 1.8 convert_bitcast_fusion
  (106 shorter events, 10.9 us)
Async XLA Ops:
  6.5 27.2 %copy-start = (bf16[512,512]{1,0:T(8,128)(2,1)S(1)}, bf16[512,512]{1,0:T(8,128)(2,1)}, u32[]{:S(2)}) copy-start(bf16[512,512]{1,0:T(8,128)(2,1)} %param.23) | copy-start | bytes 1572868
  6.5 180.2 %all-gather.12.cloned.1.call-start = ((), (), s32[]{:S(2)}) async-start(), calls=%async_computation.2 | async-start | bytes 1310720 | tf_op jit(solution)/shard_map/all_gather | solution.py:138
  19.5 169.2 %all-gather.14.cloned.1.call-start = ((), (), s32[]{:S(2)}) async-start(), calls=%async_computation.3 | async-start | bytes 1310720 | tf_op jit(solution)/shard_map/all_gather | solution.py:139
  33.7 157.6 %all-gather.10.cloned.1.call-start = ((), (), s32[]{:S(2)}) async-start(), calls=%async_computation.1 | async-start | bytes 2621440 | tf_op jit(solution)/shard_map/all_gather | solution.py:140
  33.8 43.5 %copy-start.4 = (bf16[512,128]{1,0:T(8,128)(2,1)S(1)}, bf16[512,128]{1,0:T(8,128)(2,1)}, u32[]{:S(2)}) copy-start(bf16[512,128]{1,0:T(8,128)(2,1)} %param.29) | copy-start | bytes 393220
  48.4 51.0 %copy-start.1 = (bf16[1,64,2048]{2,1,0:T(8,128)(2,1)S(1)}, bf16[1,64,2048]{2,1,0:T(8,128)(2,1)}, u32[]{:S(2)}) copy-start(bf16[1,64,2048]{2,1,0:T(8,128)(2,1)} %param.19) | copy-start | bytes 786436
  48.4 145.9 %all-gather.18.cloned.1.call-start = ((), (), s32[]{:S(2)}) async-start(), calls=%async_computation.5 | async-start | bytes 2621440 | tf_op jit(solution)/shard_map/all_gather | solution.py:142
  63.5 57.6 %copy-start.10 = (f32[2048]{0:T(1024)S(1)}, f32[2048]{0:T(1024)}, u32[]{:S(2)}) copy-start(f32[2048]{0:T(1024)} %param.20) | copy-start | bytes 24580
  63.5 149.6 %all-gather.16.cloned.1.call-start = ((), (), s32[]{:S(2)}) async-start(), calls=%async_computation.4 | async-start | bytes 2621440 | tf_op jit(solution)/shard_map/all_gather | solution.py:151
  77.2 45.6 %copy-start.5 = (bf16[512,128]{1,0:T(8,128)(2,1)S(1)}, bf16[512,128]{1,0:T(8,128)(2,1)}, u32[]{:S(2)}) copy-start(bf16[512,128]{1,0:T(8,128)(2,1)} %param.30) | copy-start | bytes 393220
  77.2 153.5 %all-gather.20.cloned.1.call-start = ((), (), s32[]{:S(2)}) async-start(), calls=%async_computation.6 | async-start | bytes 2621440 | tf_op jit(solution)/shard_map/all_gather | solution.py:152
  121.5 54.6 %copy-start.9 = (bf16[32,256]{1,0:T(8,128)(2,1)S(1)}, bf16[32,256]{1,0:T(8,128)(2,1)}, u32[]{:S(2)}) copy-start(bf16[32,256]{1,0:T(8,128)(2,1)} %param.25) | copy-start | bytes 49156
  121.5 54.6 %copy-start.11 = (f32[256]{0:T(256)S(1)}, f32[256]{0:T(256)}, u32[]{:S(2)}) copy-start(f32[256]{0:T(256)} %param.26) | copy-start | bytes 3076
  121.5 75.0 %collective-permute-start.1 = (bf16[128,128]{0,1:T(8,128)(2,1)S(1)}, bf16[128,128]{0,1:T(8,128)(2,1)S(1)}, u32[]{:S(2)}, u32[]{:S(2)}) collective-permute-start(bf16[128,128]{0,1:T(8,128)(2,1)S(1)} %convolution_convert_fusion.5), channel_id=1, source_target_pairs={{0,8},{8,16},{16,24},{1,9},{9,17},{17,25},{2,10},{10,18},{18,26},{... | collective-permute-start | bytes 98312 | tf_op jit(solution)/shard_map/ppermute | solution.py:37
  143.5 33.7 %copy-start.12 = (f32[8]{0:T(128)S(1)}, f32[8]{0:T(128)}, u32[]{:S(2)}) copy-start(f32[8]{0:T(128)} %param.31) | copy-start | bytes 100
  143.5 42.5 %copy-start.8 = (f32[128]{0:T(128)S(1)}, f32[128]{0:T(128)}, u32[]{:S(2)}) copy-start(f32[128]{0:T(128)} %param.27) | copy-start | bytes 1540
  143.5 68.5 %collective-permute-start = (bf16[128,128]{0,1:T(8,128)(2,1)}, bf16[128,128]{0,1:T(8,128)(2,1)}, u32[]{:S(2)}, u32[]{:S(2)}) collective-permute-start(bf16[128,128]{0,1:T(8,128)(2,1)} %convolution_convert_fusion.6), channel_id=1, source_target_pairs={{0,8},{8,16},{16,24},{1,9},{9,17},{17,25},{2,10},{10,18},{18,26},{... | collective-permute-start | bytes 98312 | tf_op jit(solution)/shard_map/ppermute | solution.py:37
  159.1 89.4 %reduce-scatter.2.cloned.1.call-start = ((), (), s32[]{:S(2)}) async-start(), calls=%async_computation.7 | async-start | bytes 1572864 | tf_op jit(solution)/shard_map/reduce_scatter | solution.py:215
  177.3 19.7 %copy-start.7 = (f32[2,4]{1,0:T(2,128)}, f32[2,4]{1,0:T(2,128)S(1)}, u32[]{:S(2)}) copy-start(f32[2,4]{1,0:T(2,128)S(1)} %max.30) | copy-start | bytes 100
  194.3 2.7 %copy-start.2 = (f32[2,4,64,128]{3,2,1,0:T(8,128)}, f32[2,4,64,128]{3,2,1,0:T(8,128)S(1)}, u32[]{:S(2)}) copy-start(f32[2,4,64,128]{3,2,1,0:T(8,128)S(1)} %get-tuple-element.127) | copy-start | bytes 786436
  197.1 14.1 %copy-start.3 = (f32[2,4,64,128]{3,2,1,0:T(8,128)S(1)}, f32[2,4,64,128]{3,2,1,0:T(8,128)}, u32[]{:S(2)}) copy-start(f32[2,4,64,128]{3,2,1,0:T(8,128)} %copy-done.2) | copy-start | bytes 786436
  212.0 1.3 copy-start.6
Sparse Core Ops, SparseCore 0:
  19.6 30.7 all-gather.11
  52.3 26.4 all-gather.13
  80.6 37.0 all-gather.9
  119.4 36.8 all-gather.17
  157.9 35.8 all-gather.15
  195.5 35.1 all-gather.19
  233.9 14.5 reduce-scatter.1
where the time goes:
time: 259 us; the launch traced here: 257 us
  blocking collectives  180 us (69%)
  waiting for transfers between devices  30.3 us (12%)
  matrix products  18 us (7%)
  between operations  14 us (5%)
  local copies, waits for them, and re-layouts  8.05 us (3%)
  other arithmetic  4.06 us (2%)
  starting transfers between devices  2.96 us (1%)
    all_gather x1, blocking collectives, per_device(): seq_rows = lax.all_gather(tokens, 'tp', axis=1, tiled=True)[0]  21.5 us
    all_gather x2, blocking collectives, entering_2(): pieces = jax.tree.map(lambda part: lax.all_gather(part, axis), value)  21.1 us
    all_gather x1, waiting for transfers between devices, per_device(): lax.all_gather(out_pieces[1], 'fs', axis=0, tiled=True)  15.3 us
    reduce_scatter x1, waiting for transfers between devices, per_device(): lax.psum_scatter(total + jnp.dot(window_hidden, output_maps[1], preferred...  14.7 us
    all_gather x1, blocking collectives, per_device(): lax.all_gather(quarter(gla_value_weight, 1), 'sp', axis=0, tiled=True)  14.5 us
    all_gather x1, blocking collectives, per_device(): lax.all_gather(quarter(window_query_weight, 1), 'sp', axis=0, tiled=True)  14 us
    all_gather x1, blocking collectives, per_device(): lax.all_gather(quarter(window_output_weight, 0), 'sp', axis=1, tiled=True)  13.2 us
    all_gather x1, blocking collectives, per_device(): lax.all_gather(quarter(gla_key_weight, 1), 'sp', axis=0, tiled=True)  13 us
  transfers between devices with their start and end apart: 9, of which 2 were waited for; matrix products, arithmetic and copies ran while one was open for 9% of the time, Pallas kernels for 0%

commit v1 on v0

v1 whole, which is shorter than its diff:
```python
import jax
import jax.numpy as jnp
from jax import lax
from jax.sharding import PartitionSpec as P

KEY_DIM = 64
VALUE_DIM = 128
SWA_HEADS = 16
KV_HEADS = 4
HEAD_DIM = 64
WINDOW = 128
SPAN = 64

EPS = 1e-06
SOFTMAX_TEMPER = 16.0
BF = jnp.bfloat16
F32 = jnp.float32


def rms_rows(values, gain):
    mean_square = jnp.mean(values * values, axis=-1, keepdims=True)
    return values * lax.rsqrt(mean_square + EPS) * gain


def quarter(weight, along):
    width = weight.shape[along] // lax.axis_size("fs")
    return lax.dynamic_slice_in_dim(weight, lax.axis_index("fs") * width, width, along)


def shared(weight, heads):
    group = SWA_HEADS // KV_HEADS
    first = (lax.axis_index("fs") * heads) // group
    count = max(1, heads // group)
    return lax.dynamic_slice_in_dim(weight, first * HEAD_DIM, count * HEAD_DIM, 1)


def dot(spec, a, b):
    return jnp.einsum(spec, a.astype(BF), b.astype(BF), preferred_element_type=F32)


def per_device(
    tokens,
    norm_gain,
    gla_query_weight,
    gla_key_weight,
    gla_value_weight,
    decay_down,
    decay_up,
    decay_bias,
    head_gain,
    window_query_weight,
    window_key_weight,
    window_value_weight,
    sink_logit,
    gla_output_weight,
    window_output_weight,
):
    fs, tp, sp = (lax.axis_size(n) for n in ("fs", "tp", "sp"))
    me = lax.axis_index("sp")
    heads = sink_logit.shape[0] // fs
    maps = [
        quarter(gla_value_weight, 1),
        quarter(window_query_weight, 1),
        quarter(gla_query_weight, 1),
        quarter(gla_key_weight, 1),
        shared(window_key_weight, heads),
        shared(window_value_weight, heads),
        decay_down,
    ]
    widths = [m.shape[1] for m in maps]
    w_in = lax.all_gather(jnp.concatenate(maps, 1), "sp", axis=0, tiled=True)
    w_out = lax.all_gather(
        jnp.concatenate([quarter(gla_output_weight, 0), quarter(window_output_weight, 0)], 0), "sp"
    )
    normed = rms_rows(tokens[0].astype(F32), norm_gain).astype(BF)
    normed = lax.all_gather(normed, ("fs", "tp"), axis=0, tiled=True)
    rows = normed.shape[0] // fs
    proj = jnp.dot(normed, w_in, preferred_element_type=F32).astype(BF)
    parts = []
    at = 0
    for w in widths:
        parts.append(proj[:, at : at + w])
        at += w
    gv, wq, gq, gk, wk, wv, low = parts
    up = quarter(decay_up, 1)
    logits = jnp.dot(low, up, preferred_element_type=F32) + quarter(decay_bias, 0)
    rate = jax.nn.log_sigmoid(logits) / SOFTMAX_TEMPER

    gh = gq.shape[1] // KEY_DIM
    nb = rows // SPAN
    q = gq.astype(F32).reshape(fs, nb, SPAN, gh, KEY_DIM) * KEY_DIM**-0.5
    k = gk.astype(F32).reshape(fs, nb, SPAN, gh, KEY_DIM)
    v = gv.reshape(fs, nb, SPAN, gh, VALUE_DIM)
    tri = jnp.tril(jnp.ones((SPAN, SPAN), F32))
    within = jnp.cumsum(rate.reshape(fs, nb, SPAN, gh, KEY_DIM), axis=2)
    total = within[:, :, -1]
    q_dec = q * jnp.exp(within)
    k_dec = k * jnp.exp(-within)
    k_end = k * jnp.exp(total[:, :, None] - within)
    scores = dot("bnihd,bnjhd->bnhij", q_dec, k_dec)
    scores = jnp.where(tri > 0, scores, 0.0)
    local_out = dot("bnhij,bnjhe->bnihe", scores, v)
    update = dot("bnjhd,bnjhe->bnhde", k_end, v)
    state = jnp.zeros((fs, gh, KEY_DIM, VALUE_DIM), F32)
    entering = []
    for n in range(nb):
        entering.append(state)
        state = jnp.exp(total[:, n])[..., None] * state + update[:, n]
    entering = jnp.stack(entering, 1)
    span_decay = jnp.exp(jnp.sum(total, axis=1))
    packed = jnp.concatenate([state, span_decay[..., None]], -1)
    packed = lax.all_gather(packed, "sp")

    def step(position, subtotal):
        longer = packed[position, ..., -1:] * subtotal + packed[position, ..., :-1]
        return jnp.where(position < me, longer, subtotal)

    incoming = lax.fori_loop(0, sp - 1, step, jnp.zeros_like(state))
    before = jnp.cumsum(total, axis=1) - total
    entering = entering + jnp.exp(before)[..., None] * incoming[:, None]
    gla_out = local_out + dot("bnihd,bnhde->bnihe", q_dec, entering)
    gla_hidden = rms_rows(gla_out, head_gain).astype(BF).reshape(fs * rows, gh * VALUE_DIM)

    kvh = wk.shape[1] // HEAD_DIM
    per = heads // kvh
    wb = rows // WINDOW
    kv = jnp.concatenate([wk, wv], 1).reshape(fs, rows, -1)
    edge = lax.ppermute(kv[:, rows - WINDOW :], "sp", [(i, i + 1) for i in range(sp - 1)])
    band = jnp.concatenate([edge, kv], 1)
    band = jnp.stack(
        [band[:, i * WINDOW : (i + 2) * WINDOW] for i in range(wb)], 1
    ).reshape(fs, wb, 2 * WINDOW, 2, kvh, HEAD_DIM)
    qw = wq.reshape(fs, wb, WINDOW, kvh, per, HEAD_DIM)
    s = dot("bnqhgd,bnkhd->bnhgqk", qw, band[:, :, :, 0]) * HEAD_DIM**-0.5
    distance = jnp.arange(WINDOW)[:, None] + WINDOW - jnp.arange(2 * WINDOW)[None, :]
    where = me * rows + jnp.arange(wb)[:, None, None] * WINDOW - WINDOW + jnp.arange(2 * WINDOW)
    valid = ((distance >= 0) & (distance < WINDOW))[None] & (where >= 0)
    s = jnp.where(valid[None, :, None, None], s, -1e30)
    sink = quarter(sink_logit, 0).reshape(1, 1, kvh, per, 1, 1)
    top = jnp.maximum(jnp.max(s, -1, keepdims=True), sink)
    e = jnp.exp(s - top)
    weights = (e / (jnp.sum(e, -1, keepdims=True) + jnp.exp(sink - top))).astype(BF)
    hidden = dot("bnhgqk,bnkhd->bnqhgd", weights, band[:, :, :, 1]).astype(BF)
    hidden = hidden.reshape(fs * rows, heads * HEAD_DIM)

    both = jnp.concatenate([gla_hidden, hidden], 1)
    part = jnp.einsum("rk,skn->rsn", both, w_out, preferred_element_type=F32)
    part = part.reshape(fs * rows, -1)
    mixed = lax.psum_scatter(part, ("fs", "tp"), scatter_dimension=0, tiled=True)
    return mixed.astype(BF)[None]


def solution(mesh):
    in_specs = (
        P("fs", ("sp", "tp"), None),
        P(),
        P("sp", "tp"),
        P("sp", "tp"),
        P("sp", "tp"),
        P("sp", None),
        P(None, "tp"),
        P("tp"),
        P(),
        P("sp", "tp"),
        P("sp", "tp"),
        P("sp", "tp"),
        P("tp"),
        P("tp", "sp"),
        P("tp", "sp"),
    )
    out_specs = P("fs", ("sp", "tp"), None)
    return jax.shard_map(
        per_device, mesh=mesh, in_specs=in_specs, out_specs=out_specs, check_vma=False
    )
```

time: 259 us -> 220 us (0.85)
  blocking collectives: 180 us -> 38.6 us
  waiting for transfers between devices: 30.3 us -> 133 us
  matrix products: 18 us -> 9.7 us
  local copies, waits for them, and re-layouts: 8.05 us -> 16.2 us
    all_gather x15 -> x1, blocking collectives: 180 us -> 38.6 us  [per_device(): packed = lax.all_gather(packed, 'sp')]
    all_gather x6 -> x3, waiting for transfers between devices: 15.4 us -> 81.5 us  [the longest x1 50.3 us: per_device(): w_in = lax.all_gather(jnp.concatenate(maps, 1), 'sp', axis=0, tiled=True)]
    reduce_scatter x1, waiting for transfers between devices: 14.7 us -> 51.7 us  [per_device(): lax.psum_scatter(part, ('fs', 'tp'), scatter_dimension=0, tiled=True)]
    dot_general x15 -> x8, matrix products: 18 us -> 9.7 us  [the longest x1 3.94 us: per_device(): part = jnp.einsum('rk,skn->rsn', both, w_out, preferred_element_type=F32)]
    reshape x0 -> x6, local copies, waits for them, and re-layouts: none -> 6.68 us  [the longest x1 5.43 us: per_device(): part = part.reshape(fs * rows, -1)]
    dynamic_slice x9 -> x6, local copies, waits for them, and re-layouts: 5.8 us -> 4.37 us  [the longest x5 3.26 us: quarter(): lax.dynamic_slice_in_dim(weight, lax.axis_index('fs') * width, width, along)]
  transfers between devices with their start and end apart: 9 -> 5, of which waited for: 2 -> 3; matrix products, arithmetic and copies ran while one was open for 9% -> 7% of each run, Pallas kernels for 0% -> 0%
where the time goes in v1:
time: 220 us; the launch traced here: 218 us
  waiting for transfers between devices  133 us (60%)
  blocking collectives  38.6 us (18%)
  local copies, waits for them, and re-layouts  16.2 us (7%)
  between operations  13.5 us (6%)
  matrix products  9.7 us (4%)
  other arithmetic  5.13 us (2%)
    reduce_scatter x1, waiting for transfers between devices, per_device(): lax.psum_scatter(part, ('fs', 'tp'), scatter_dimension=0, tiled=True)  51.7 us
    all_gather x1, waiting for transfers between devices, per_device(): w_in = lax.all_gather(jnp.concatenate(maps, 1), 'sp', axis=0, tiled=True)  50.3 us
    all_gather x1, blocking collectives, per_device(): packed = lax.all_gather(packed, 'sp')  38.6 us
    all_gather x1, waiting for transfers between devices, per_device(): normed = lax.all_gather(normed, ('fs', 'tp'), axis=0, tiled=True)  31.2 us
    reshape x1, local copies, waits for them, and re-layouts, per_device(): part = part.reshape(fs * rows, -1)  5.43 us
  transfers between devices with their start and end apart: 5, of which 3 were waited for; matrix products, arithmetic and copies ran while one was open for 7% of the time, Pallas kernels for 0%

profile of v1, /device:TPU:25, one launch (start us, length us, event | category | flops | bytes accessed | tf_op | source)
XLA Modules:
  0.0 217.9 jit_solution(4197163426944656206)
XLA Ops:
  6.5 0.9 copy.54
  7.5 1.1 constant_dynamic-slice_fusion.2
  8.6 1.1 constant_dynamic-slice_fusion.4
  9.7 1.0 constant_dynamic-slice_fusion.6
  10.7 1.1 concatenate.23
  12.1 0.8 fusion.11
  13.0 1.0 constant_dynamic-slice_fusion
  14.0 0.7 pad_maximum_fusion
  15.1 50.3 %all-gather.8.cloned.1.call-done = bf16[2048,544]{1,0:T(8,128)(2,1)} async-done(((bf16[512,544]{1,0:T(8,128)(2,1)}), bf16[2048,544]{1,0:T(8,128)(2,1)}) %all-gather.8.cloned.1.call-update) | async-done | bytes 2228240 | tf_op jit(solution)/shard_map/all_gather | solution.py:71
  65.4 31.2 %all-gather.6.cloned.1.call-done = bf16[512,2048]{1,0:T(8,128)(2,1)} async-done(((bf16[64,2048]{1,0:T(8,128)(2,1)}), bf16[512,2048]{1,0:T(8,128)(2,1)}) %all-gather.6.cloned.1.call-update) | async-done | bytes 2097168 | tf_op jit(solution)/shard_map/all_gather | solution.py:76
  96.6 3.8 %convolution_convert_fusion = bf16[512,544]{0,1:T(8,128)(2,1)S(1)} fusion(bf16[512,2048]{1,0:T(8,128)(2,1)} %all-gather.6.cloned.1.call-done, bf16[2048,544]{1,0:T(8,128)(2,1)} %all-gather.8.cloned.1.call-done), kind=kOutput, calls=%fused_computation.5 | convolution fusion | flops 1141129216 | bytes 4882432 | tf_op jit(solution)/shard_map/dot_general | solution.py:78
  100.5 0.4 fusion.18
  101.0 0.2 fusion.38
  101.6 0.7 copy.100
  102.3 0.7 reshape.337
  103.2 1.3 collective-permute-start
  104.5 0.2 convolution_bitcast_fusion
  105.0 38.6 %all-gather = f32[16,1,64,129]{3,2,1,0:T(8,128)S(1)} all-gather(f32[4,1,64,129]{3,2,1,0:T(8,128)S(1)} %maximum_bitcast_fusion), channel_id=2, replica_groups=mesh['sp'=4,'fs'=4,'tp'=2] {'sp'}, dimensions={0}, use_global_device_ids=true | all-gather | bytes 660480 | tf_op jit(solution)/shard_map/all_gather | solution.py:112
  143.7 0.9 copy.65
  144.5 0.6 while.14
  144.7 0.2 fusion.50
  145.2 0.3 fusion.6
  145.6 0.4 multiply_reduce_fusion
  146.1 0.9 copy_dynamic-update-slice_fusion.1
  147.1 0.4 fusion.37
  147.5 0.2 fusion.8
  147.8 0.3 fusion.5
  148.1 0.2 copy.84
  148.5 3.9 %fusion.13 = f32[512,4,512]{0,2,1:T(8,128)} fusion(bf16[4,256,512]{2,1,0:T(8,128)(2,1)} %bitcast.124, bf16[512,128]{1,0:T(8,128)(2,1)S(1)} %reshape.349, bf16[512,128]{1,0:T(8,128)(2,1)S(1)} %bitcast.125), kind=kOutput, calls=%fused_computation.29 | convolution fusion | flops 537395200 | bytes 5505024 | tf_op jit(solution)/shard_map/rk,skn->rsn/dot_general | solution.py:147
  152.4 5.4 %copy.76 = f32[512,2048]{1,0:T(8,128)} copy(f32[512,2048]{0,1:T(8,128)} %bitcast.112) | data formatting | bytes 8388608 | tf_op jit(solution)/shard_map/reshape | solution.py:148
  157.9 51.7 %reduce-scatter.2.cloned.1.call-done = f32[64,2048]{1,0:T(8,128)} async-done(((f32[512,2048]{1,0:T(8,128)}), f32[64,2048]{1,0:T(8,128)}) %reduce-scatter.2.cloned.1.call-update) | async-done | bytes 524304 | tf_op jit(solution)/shard_map/reduce_scatter | solution.py:149
  209.6 1.8 convert_bitcast_fusion
  (64 shorter events, 2.7 us)
Async XLA Ops:
  6.5 93.9 %copy-start = (bf16[32,256]{1,0:T(8,128)(2,1)S(1)}, bf16[32,256]{1,0:T(8,128)(2,1)}, u32[]{:S(2)}) copy-start(bf16[32,256]{1,0:T(8,128)(2,1)} %param.23) | copy-start | bytes 49156
  6.5 5.4 %copy-start.1 = (bf16[1,64,2048]{2,1,0:T(8,128)(2,1)S(1)}, bf16[1,64,2048]{2,1,0:T(8,128)(2,1)}, u32[]{:S(2)}) copy-start(bf16[1,64,2048]{2,1,0:T(8,128)(2,1)} %param.17) | copy-start | bytes 786436
  6.5 58.9 %all-gather.8.cloned.1.call-start = ((), (), s32[]{:S(2)}) async-start(), calls=%async_computation.2 | async-start | bytes 3276800 | tf_op jit(solution)/shard_map/all_gather | solution.py:71
  6.5 5.5 %copy-start.3 = (f32[2048]{0:T(1024)S(1)}, f32[2048]{0:T(1024)}, u32[]{:S(2)}) copy-start(f32[2048]{0:T(1024)} %param.18) | copy-start | bytes 24580
  10.7 4.1 %copy-start.5 = (f32[256]{0:T(256)S(1)}, f32[256]{0:T(256)}, u32[]{:S(2)}) copy-start(f32[256]{0:T(256)} %param.24) | copy-start | bytes 3076
  10.7 4.2 %copy-start.6 = (f32[8]{0:T(128)S(1)}, f32[8]{0:T(128)}, u32[]{:S(2)}) copy-start(f32[8]{0:T(128)} %param.29) | copy-start | bytes 100
  11.8 84.7 %all-gather.6.cloned.1.call-start = ((), (), s32[]{:S(2)}) async-start(), calls=%async_computation.1 | async-start | bytes 2359296 | tf_op jit(solution)/shard_map/all_gather | solution.py:76
  12.9 135.5 %all-gather.10.cloned.1.call-start = ((), (), s32[]{:S(2)}) async-start(), calls=%async_computation.4 | async-start | bytes 1310720 | tf_op jit(solution)/shard_map/all_gather | solution.py:72
  14.7 194.8 %reduce-scatter.2.cloned.1.call-start = ((), (), s32[]{:S(2)}) async-start(), calls=%async_computation.3 | async-start | bytes 4718592 | tf_op jit(solution)/shard_map/reduce_scatter | solution.py:149
  103.2 42.9 %collective-permute-start = (bf16[4,128,128]{1,2,0:T(8,128)(2,1)}, bf16[4,128,128]{1,2,0:T(8,128)(2,1)}, u32[]{:S(2)}, u32[]{:S(2)}) collective-permute-start(bf16[4,128,128]{1,2,0:T(8,128)(2,1)} %bitcast.104), channel_id=1, source_target_pairs={{0,8},{8,16},{16,24},{1,9},{9,17},{17,25},{2,10},{10,18},{18,26},{... | collective-permute-start | bytes 393224 | tf_op jit(solution)/shard_map/ppermute | solution.py:128
  145.1 0.9 copy-start.4
  145.1 2.0 copy-start.2
Sparse Core Ops, SparseCore 0:
  12.0 53.4 all-gather.7
  67.3 29.2 all-gather.5
  98.2 39.2 all-gather.9
  158.0 51.5 reduce-scatter.1

commit v2 on v1

v2 whole, which is shorter than its diff:
```python
import functools

import jax
import jax.numpy as jnp
from jax import lax
from jax.experimental import pallas as pl
from jax.experimental.pallas import tpu as pltpu
from jax.sharding import PartitionSpec as P

KEY_DIM = 64
VALUE_DIM = 128
SWA_HEADS = 16
KV_HEADS = 4
HEAD_DIM = 64
WINDOW = 128
SPAN = 64

EPS = 1e-06
SOFTMAX_TEMPER = 16.0
BF = jnp.bfloat16
F32 = jnp.float32


def rms_rows(values, gain):
    mean_square = jnp.mean(values * values, axis=-1, keepdims=True)
    return values * lax.rsqrt(mean_square + EPS) * gain


def quarter(weight, along):
    width = weight.shape[along] // lax.axis_size("fs")
    return lax.dynamic_slice_in_dim(weight, lax.axis_index("fs") * width, width, along)


def shared(weight, heads):
    group = SWA_HEADS // KV_HEADS
    first = (lax.axis_index("fs") * heads) // group
    count = max(1, heads // group)
    return lax.dynamic_slice_in_dim(weight, first * HEAD_DIM, count * HEAD_DIM, 1)


def nt(a, b):
    return lax.dot_general(a, b, (((1,), (1,)), ((), ())), preferred_element_type=F32)


def nn(a, b):
    return lax.dot_general(a, b, (((1,), (0,)), ((), ())), preferred_element_type=F32)


def tn(a, b):
    return lax.dot_general(a, b, (((0,), (0,)), ((), ())), preferred_element_type=F32)


def exact(a, b):
    return lax.dot_general(
        a, b, (((1,), (0,)), ((), ())), precision=lax.Precision.HIGHEST, preferred_element_type=F32
    )


def mixer_kernel(
    sizes,
    tok_ref,
    win_ref,
    low_ref,
    wout_ref,
    ngain_ref,
    up_ref,
    bias_ref,
    hgain_ref,
    sink_ref,
    out_ref,
    x_buf,
    w_buf,
    l_buf,
    o_buf,
    proj,
    edge_out,
    edge_in,
    state_out,
    state_in,
    local_out,
    q_far,
    hidden,
    half_out,
    half_in,
    half_own,
    piece_out,
    piece_in,
    piece_own,
    local_sem,
    tok_send,
    tok_recv,
    w_send,
    w_recv,
    l_send,
    l_recv,
    o_send,
    o_recv,
    edge_sem,
    state_send,
    state_recv,
    half_send,
    half_recv,
    piece_send,
    piece_recv,
):
    sp, fs, tp = sizes
    me = lax.axis_index("sp")
    f = lax.axis_index("fs")
    c = lax.axis_index("tp")
    plane = fs * tp
    mine = f * tp + c
    own = tok_ref.shape[0]
    rows = own * tp
    kc = win_ref.shape[0]
    MESH = pl.DeviceIdType.MESH

    def remote(src, dst, ssem, rsem, target):
        return pltpu.make_async_remote_copy(
            src_ref=src, dst_ref=dst, send_sem=ssem, recv_sem=rsem,
            device_id=target, device_id_type=MESH,
        )

    def w_rows(s):
        return w_buf.at[pl.ds(pl.multiple_of(s * kc, kc), kc)]

    def w_copy(s, way, first):
        target = {"sp": me + (1 if way == 0 else -1)}
        return remote(
            win_ref if first else w_rows(s), w_rows(s), w_send.at[way, s], w_recv.at[s], target
        )

    def l_copy(s, way, first):
        target = {"sp": me + (1 if way == 0 else -1)}
        return remote(
            low_ref if first else l_buf.at[s], l_buf.at[s], l_send.at[way, s], l_recv.at[s], target
        )

    def o_copy(s, way, first):
        target = {"sp": me + (1 if way == 0 else -1)}
        return remote(
            wout_ref if first else o_buf.at[s], o_buf.at[s], o_send.at[way, s], o_recv.at[s], target
        )

    def tok_rows(i):
        return x_buf.at[pl.ds(pl.multiple_of(i * own, own), own)]

    def tok_copy(d, peer, sender):
        return remote(
            tok_ref, tok_rows(sender), tok_send.at[d - 1], tok_recv.at[d - 1],
            {"fs": peer // tp, "tp": peer % tp},
        )

    locals_ = [
        pltpu.make_async_copy(win_ref, w_rows(me), local_sem.at[0]),
        pltpu.make_async_copy(low_ref, l_buf.at[me], local_sem.at[1]),
        pltpu.make_async_copy(wout_ref, o_buf.at[me], local_sem.at[2]),
        pltpu.make_async_copy(tok_ref, tok_rows(mine), local_sem.at[3]),
    ]

    def sends(k):
        @pl.when((me - k >= 0) & (me + 1 < sp))
        def _():
            l_copy(me - k, 0, k == 0).start()
            w_copy(me - k, 0, k == 0).start()

        @pl.when((me + k < sp) & (me >= 1))
        def _():
            l_copy(me + k, 1, k == 0).start()
            w_copy(me + k, 1, k == 0).start()

        @pl.when((me == k) & (me + 1 < sp))
        def _():
            o_copy(me, 0, True).start()

        @pl.when((sp - 1 - me == k) & (me >= 1))
        def _():
            o_copy(me, 1, True).start()

    for k in range(sp - 1):
        sends(k)
        if k == 0:
            for d in range(1, plane):
                tok_copy(d, lax.rem(mine + d, plane), mine).start()
            for copy in locals_:
                copy.start()

        @pl.when(me - 1 - k >= 0)
        def _():
            l_copy(me - 1 - k, 0, False).wait_recv()
            w_copy(me - 1 - k, 0, False).wait_recv()

        @pl.when(me + 1 + k < sp)
        def _():
            l_copy(me + 1 + k, 1, False).wait_recv()
            w_copy(me + 1 + k, 1, False).wait_recv()

    inner = (me >= 1) & (me + 1 < sp)
    for k in range(1, sp - 1):
        @pl.when(inner & (me - k >= 0))
        def _():
            o_copy(me - k, 0, False).wait_recv()
            o_copy(me - k, 0, False).start()

        @pl.when(inner & (me + k < sp))
        def _():
            o_copy(me + k, 1, False).wait_recv()
            o_copy(me + k, 1, False).start()

    for copy in locals_:
        copy.wait()
    for d in range(1, plane):
        tok_copy(d, mine, lax.rem(mine + plane - d, plane)).wait_recv()

    cols = [VALUE_DIM, 2 * HEAD_DIM, KEY_DIM, KEY_DIM, HEAD_DIM, HEAD_DIM]
    starts = [sum(cols[:i]) for i in range(len(cols))]

    def project(b, _):
        x = x_buf[pl.ds(pl.multiple_of(b * rows, rows), rows)].astype(F32)
        normed = rms_rows(x, ngain_ref[...]).astype(BF)
        p = nn(normed, w_buf[...]).astype(BF)
        proj[b, :, : p.shape[1]] = p
        edge_out[b] = p[rows - WINDOW :, starts[4] : starts[4] + 2 * HEAD_DIM]
        low = nt(normed[:, :kc], l_buf[0])
        for s in range(1, sp):
            low += nt(normed[:, s * kc : (s + 1) * kc], l_buf[s])
        proj[b, :, p.shape[1] : p.shape[1] + low.shape[1]] = low.astype(BF)
        return 0

    lax.fori_loop(0, fs, project, 0)
    edge = remote(edge_out, edge_in, edge_sem.at[0], edge_sem.at[1], {"sp": me + 1})

    @pl.when(me + 1 < sp)
    def _():
        edge.start()

    @pl.when(me == 0)
    def _():
        edge_in[...] = jnp.zeros_like(edge_in)

    nb = rows // SPAN
    low_at = sum(cols)
    lower = (
        lax.broadcasted_iota(jnp.int32, (SPAN, SPAN), 0)
        >= lax.broadcasted_iota(jnp.int32, (SPAN, SPAN), 1)
    )
    tri = lower.astype(F32)
    for b in range(fs):
        low = proj[b, :, low_at : low_at + up_ref.shape[0]]
        z = nn(low, up_ref[...]) + bias_ref[...]
        rate = (jnp.minimum(z, 0.0) - jnp.log1p(jnp.exp(-jnp.abs(z)))) / SOFTMAX_TEMPER
        state = None
        before = jnp.zeros((1, KEY_DIM), F32)
        for n in range(nb):
            r0 = n * SPAN
            within = exact(tri, rate[r0 : r0 + SPAN])
            total = within[SPAN - 1 :]
            v = proj[b, r0 : r0 + SPAN, starts[0] : starts[0] + VALUE_DIM]
            q = proj[b, r0 : r0 + SPAN, starts[2] : starts[2] + KEY_DIM].astype(F32)
            k = proj[b, r0 : r0 + SPAN, starts[3] : starts[3] + KEY_DIM].astype(F32)
            q_dec = q * KEY_DIM**-0.5 * jnp.exp(within)
            k_dec = (k * jnp.exp(-within)).astype(BF)
            k_end = (k * jnp.exp(total - within)).astype(BF)
            scores = jnp.where(lower, nt(q_dec.astype(BF), k_dec), 0.0)
            o = nn(scores.astype(BF), v)
            if state is not None:
                o += nt(q_dec.astype(BF), state.astype(BF))
            local_out[b, r0 : r0 + SPAN] = o
            q_far[b, r0 : r0 + SPAN] = (q_dec * jnp.exp(before)).astype(BF)
            update = tn(v, k_end)
            state = update if state is None else jnp.exp(total) * state + update
            before = before + total
        half = (b % 2) * KEY_DIM
        state_out[b // 2, :VALUE_DIM, half : half + KEY_DIM] = state.astype(BF)
        state_out[b // 2, VALUE_DIM:, half : half + KEY_DIM] = jnp.broadcast_to(
            jnp.exp(before), (16, KEY_DIM)
        ).astype(BF)

    def state_copy(d, sender):
        return remote(
            state_out, state_in.at[sender], state_send.at[d - 1], state_recv.at[sender],
            {"sp": me + d},
        )

    for d in range(1, sp):
        @pl.when(me + d < sp)
        def _():
            state_copy(d, me).start()

    @pl.when(me >= 1)
    def _():
        edge.wait_recv()

    qi = lax.broadcasted_iota(jnp.int32, (WINDOW, 2 * WINDOW), 0)
    ki = lax.broadcasted_iota(jnp.int32, (WINDOW, 2 * WINDOW), 1)
    distance = qi + WINDOW - ki
    inside = (distance >= 0) & (distance < WINDOW)
    heads = sink_ref.shape[1]
    for b in range(fs):
        for w in range(rows // WINDOW):
            r0 = w * WINDOW
            here = proj[b, r0 : r0 + WINDOW, starts[4] : starts[4] + 2 * HEAD_DIM]
            if w == 0:
                past = edge_in[b]
                valid = inside & ((ki >= WINDOW) | (me >= 1))
            else:
                past = proj[b, r0 - WINDOW : r0, starts[4] : starts[4] + 2 * HEAD_DIM]
                valid = inside
            band = jnp.concatenate([past, here], 0)
            bk = band[:, :HEAD_DIM]
            bv = band[:, HEAD_DIM:]
            for h in range(heads):
                q0 = starts[1] + h * HEAD_DIM
                q = proj[b, r0 : r0 + WINDOW, q0 : q0 + HEAD_DIM]
                s = jnp.where(valid, nt(q, bk) * HEAD_DIM**-0.5, -1e30)
                sink = sink_ref[0:1, h : h + 1]
                top = jnp.maximum(jnp.max(s, -1, keepdims=True), sink)
                e = jnp.exp(s - top)
                den = jnp.sum(e, -1, keepdims=True) + jnp.exp(sink - top)
                a = nn((e / den).astype(BF), bv).astype(BF)
                h0 = VALUE_DIM + h * HEAD_DIM
                hidden[b, r0 : r0 + WINDOW, h0 : h0 + HEAD_DIM] = a

    for i in range(sp - 1):
        @pl.when(i < me)
        def _():
            state_copy(1, i).wait_recv()

        @pl.when(i >= me)
        def _():
            state_in[i] = jnp.zeros(state_in.shape[1:], BF)

    for b in range(fs):
        half = (b % 2) * KEY_DIM
        incoming = jnp.zeros((VALUE_DIM, KEY_DIM), F32)
        for i in range(sp - 1):
            got = state_in[i, b // 2, :VALUE_DIM, half : half + KEY_DIM].astype(F32)
            kept = state_in[i, b // 2, VALUE_DIM : VALUE_DIM + 1, half : half + KEY_DIM].astype(F32)
            incoming = jnp.where(i < me, kept * incoming + got, incoming)
        o = local_out[b] + nt(q_far[b], incoming.astype(BF))
        hidden[b, :, :VALUE_DIM] = rms_rows(o, hgain_ref[...]).astype(BF)

    forward = 2 * me < sp
    nc = o_buf.shape[2]

    def chunk(t):
        return lax.rem(jnp.where(forward, me + t, me - t) + sp, sp)

    def half_copy(s):
        return remote(half_out.at[s], half_in.at[s], half_send.at[s], half_recv.at[s], {"tp": 1 - c})

    def piece_copy(s, d, target):
        return remote(
            piece_out.at[s, d - 1], piece_in.at[s, d - 1],
            piece_send.at[s, d - 1], piece_recv.at[s, d - 1], {"fs": target},
        )

    def produce(t):
        s = chunk(t)

        @pl.when(jnp.logical_not(inner) & (t > 0))
        def _():
            o_copy(s, 0, False).wait_recv()

        w = o_buf[s]
        for b in range(fs):
            part = nn(hidden[b], w)
            lo, hi = part[:own], part[own:]
            half_out[s, b] = jnp.where(c == 0, hi, lo).astype(BF)
            half_own[s, b] = jnp.where(c == 0, lo, hi)
        half_copy(s).start()

    def combine(t):
        s = chunk(t)
        half_copy(s).wait_recv()
        for d in range(1, fs):
            to = lax.rem(f + d, fs)
            piece_out[s, d - 1] = (half_own[s, to] + half_in[s, to].astype(F32)).astype(BF)
            piece_copy(s, d, to).start()
        piece_own[s] = half_own[s, f] + half_in[s, f].astype(F32)

    def finish(t):
        s = chunk(t)
        total = piece_own[s]
        for d in range(1, fs):
            piece_copy(s, d, f).wait_recv()
            total += piece_in[s, d - 1].astype(F32)
        out_ref[s] = total.astype(BF)

    produce(0)

    def steady(t, _):
        produce(t)
        combine(t - 1)
        return 0

    lax.fori_loop(1, sp, steady, 0)
    combine(sp - 1)

    def close(t, _):
        finish(t)
        s = chunk(t)
        half_copy(s).wait_send()
        for d in range(1, fs):
            piece_copy(s, d, f).wait_send()
        return 0

    lax.fori_loop(0, sp, close, 0)

    for k in range(sp - 1):
        @pl.when((me - k >= 0) & (me + 1 < sp))
        def _():
            l_copy(me - k, 0, False).wait_send()
            w_copy(me - k, 0, False).wait_send()
            o_copy(me - k, 0, False).wait_send()

        @pl.when((me + k < sp) & (me >= 1))
        def _():
            l_copy(me + k, 1, False).wait_send()
            w_copy(me + k, 1, False).wait_send()
            o_copy(me + k, 1, False).wait_send()

    for d in range(1, plane):
        tok_copy(d, mine, mine).wait_send()

    @pl.when(me + 1 < sp)
    def _():
        edge.wait_send()

    for d in range(1, sp):
        @pl.when(me + d < sp)
        def _():
            state_copy(d, me).wait_send()


def per_device(
    tokens,
    norm_gain,
    gla_query_weight,
    gla_key_weight,
    gla_value_weight,
    decay_down,
    decay_up,
    decay_bias,
    head_gain,
    window_query_weight,
    window_key_weight,
    window_value_weight,
    sink_logit,
    gla_output_weight,
    window_output_weight,
):
    fs, tp, sp = (lax.axis_size(n) for n in ("fs", "tp", "sp"))
    heads = sink_logit.shape[0] // fs
    w_in = jnp.concatenate(
        [
            quarter(gla_value_weight, 1),
            quarter(window_query_weight, 1),
            quarter(gla_query_weight, 1),
            quarter(gla_key_weight, 1),
            shared(window_key_weight, heads),
            shared(window_value_weight, heads),
        ],
        1,
    )
    low = decay_down.T
    w_out = jnp.concatenate([quarter(gla_output_weight, 0), quarter(window_output_weight, 0)], 0)
    own = tokens.shape[1]
    rows = own * tp
    kc, width = w_in.shape
    rank = low.shape[0]
    depth, nc = w_out.shape
    vm = pltpu.VMEM
    dma = pltpu.SemaphoreType.DMA
    scratch = [
        vm((fs * rows, tokens.shape[2]), BF),
        vm((sp * kc, width), BF),
        vm((sp, rank, kc), BF),
        vm((sp, depth, nc), BF),
        vm((fs, rows, width + 128), BF),
        vm((fs, WINDOW, 2 * HEAD_DIM), BF),
        vm((fs, WINDOW, 2 * HEAD_DIM), BF),
        vm((fs // 2, VALUE_DIM + 16, 2 * KEY_DIM), BF),
        vm((sp, fs // 2, VALUE_DIM + 16, 2 * KEY_DIM), BF),
        vm((fs, rows, VALUE_DIM), F32),
        vm((fs, rows, KEY_DIM), BF),
        vm((fs, rows, depth), BF),
        vm((sp, fs, own, nc), BF),
        vm((sp, fs, own, nc), BF),
        vm((sp, fs, own, nc), F32),
        vm((sp, fs - 1, own, nc), BF),
        vm((sp, fs - 1, own, nc), BF),
        vm((sp, own, nc), F32),
        dma((4,)),
        dma((fs * tp - 1,)),
        dma((fs * tp - 1,)),
        dma((2, sp)),
        dma((sp,)),
        dma((2, sp)),
        dma((sp,)),
        dma((2, sp)),
        dma((sp,)),
        dma((2,)),
        dma((sp,)),
        dma((sp,)),
        dma((sp,)),
        dma((sp,)),
        dma((sp, fs - 1)),
        dma((sp, fs - 1)),
    ]
    spec = pl.BlockSpec(memory_space=pltpu.VMEM)
    mixed = pl.pallas_call(
        functools.partial(mixer_kernel, (sp, fs, tp)),
        out_shape=jax.ShapeDtypeStruct((sp, own, nc), BF),
        in_specs=[spec] * 9,
        out_specs=spec,
        scratch_shapes=scratch,
        compiler_params=pltpu.CompilerParams(
            has_side_effects=True, vmem_limit_bytes=60 * 1024 * 1024
        ),
    )(
        tokens[0],
        w_in,
        low,
        w_out,
        norm_gain[None],
        quarter(decay_up, 1),
        quarter(decay_bias, 0)[None],
        head_gain[None],
        quarter(sink_logit, 0)[None],
    )
    return mixed.transpose(1, 0, 2).reshape(1, own, sp * nc)


def solution(mesh):
    in_specs = (
        P("fs", ("sp", "tp"), None),
        P(),
        P("sp", "tp"),
        P("sp", "tp"),
        P("sp", "tp"),
        P("sp", None),
        P(None, "tp"),
        P("tp"),
        P(),
        P("sp", "tp"),
        P("sp", "tp"),
        P("sp", "tp"),
        P("tp"),
        P("tp", "sp"),
        P("tp", "sp"),
    )
    out_specs = P("fs", ("sp", "tp"), None)
    return jax.shard_map(
        per_device, mesh=mesh, in_specs=in_specs, out_specs=out_specs, check_vma=False
    )
```

time: 220 us -> 100 us (0.45); the launches traced: 218 us -> 100 us
  waiting for transfers between devices: 133 us -> 0 us
  Pallas kernels: 0 us -> 90.3 us
  blocking collectives: 38.6 us -> 0 us
  between operations: 13.5 us -> 0.06 us
  matrix products: 9.7 us -> 0 us
  local copies, waits for them, and re-layouts: 16.2 us -> 8.99 us
  other arithmetic: 5.13 us -> 0.72 us
    pallas_call x0 -> x1, Pallas kernels: none -> 90.3 us  [per_device(): pl.pallas_call(functools.partial(mixer_kernel, (sp, fs, tp)), out_shape=j...]
    all_gather x3 -> x0, waiting for transfers between devices: 81.5 us -> none  [the longest x1 50.3 us: per_device(): w_in = lax.all_gather(jnp.concatenate(maps, 1), 'sp', axis=0, tiled=True)]
    reduce_scatter x1 -> x0, waiting for transfers between devices: 51.7 us -> none  [per_device(): lax.psum_scatter(part, ('fs', 'tp'), scatter_dimension=0, tiled=True)]
    all_gather x1 -> x0, blocking collectives: 38.6 us -> none  [per_device(): packed = lax.all_gather(packed, 'sp')]
    dot_general x8 -> x0, matrix products: 9.7 us -> none  [the longest x1 3.94 us: per_device(): part = jnp.einsum('rk,skn->rsn', both, w_out, preferred_element_type=F32)]
    reshape x6 -> x1, local copies, waits for them, and re-layouts: 6.68 us -> 0.88 us  [per_device(): return mixed.transpose(1, 0, 2).reshape(1, own, sp * nc)]
  transfers between devices with their start and end apart: 5 -> 0, of which waited for: 3 -> 0; matrix products, arithmetic and copies ran while one was open for 7% -> 0% of each run, Pallas kernels for 0% -> 0%
where the time goes in v2:
time: 100 us
  Pallas kernels  90.3 us (90%)
  local copies, waits for them, and re-layouts  8.99 us (9%)
    pallas_call x1, Pallas kernels, per_device(): pl.pallas_call(functools.partial(mixer_kernel, (sp, fs, tp)), out_shape=j...  90.3 us
    dynamic_slice x4, local copies, waits for them, and re-layouts, quarter(): lax.dynamic_slice_in_dim(weight, lax.axis_index('fs') * width, width, along)  2.79 us

profile of v2, /device:TPU:25, one launch (start us, length us, event | category | flops | bytes accessed | tf_op | source)
XLA Modules:
  0.0 100.1 jit_solution(1547629721912928105)
XLA Ops:
  0.0 0.0 copy-start
  0.0 0.0 copy-start.1
  0.0 0.0 copy-start.2
  0.0 1.2 %constant_dynamic-slice_fusion.3 = (bf16[512,64]{1,0:T(8,128)(2,1)S(1)}, bf16[512,64]{1,0:T(8,128)(2,1)S(1)}) fusion(bf16[512,128]{1,0:T(8,128)(2,1)} %param.26, s32[]{:T(128)S(6)} %select_n.28, bf16[512,128]{1,0:T(8,128)(2,1)} %param.25), kind=kLoop, calls=%fused_computation.4 | loop fusion | bytes 262148 | tf_op jit(solution)/shard_map/dynamic_slice | solution.py:38
  1.2 0.0 copy-done.1
  1.2 0.0 copy-done.2
  1.2 0.1 constant_dynamic-slice_fusion.5
  1.4 1.0 constant_dynamic-slice_fusion.7
  2.4 1.1 %concatenate.6.win_ref = bf16[512,512]{1,0:T(8,128)(2,1)} concatenate(bf16[512,128]{1,0:T(8,128)(2,1)S(1)} %get-tuple-element.8, bf16[512,128]{1,0:T(8,128)(2,1)S(1)} %get-tuple-element.7, bf16[512,64]{1,0:T(8,128)(2,1)S(1)} %get-tuple-element.10, bf16[512,64]{1,0:T(8,128)(2,1)S(1)} %get-tuple-element.9, bf16[512,64]{1,0:T(8,128)(2,1)S(1)} %get-tuple-element.12, ...), dimensions={1} | concatenate | bytes 1048576 | tf_op jit(solution)/shard_map/concatenate | solution.py:454
  3.4 1.0 constant_dynamic-slice_fusion.1
  4.4 0.7 pad_maximum_fusion.wout_ref
  5.1 0.0 copy-start.4
  5.1 0.7 copy-done.4
  5.8 0.6 dynamic-slice_bitcast_fusion.sink_ref
  6.4 0.0 copy-done
  6.4 0.0 copy-start.3
  6.4 0.7 constant_dynamic-slice_fusion.up_ref
  7.1 0.0 copy-done.3
  7.1 0.6 dynamic-slice_bitcast_fusion.1.bias_ref
  7.7 90.3 %shard_map.145 = bf16[4,64,512]{2,1,0:T(8,128)(2,1)} custom-call(bf16[64,2048]{1,0:T(8,128)(2,1)} %bitcast.10, bf16[512,512]{1,0:T(8,128)(2,1)} %concatenate.6.win_ref, bf16[32,512]{1,0:T(8,128)(2,1)} %bitcast.11, bf16[256,512]{1,0:T(8,128)(2,1)} %pad_maximum_fusion.wout_ref, f32[1,2048]{1,0:T(1,128)} %bitcast.12, ...), custom_call_target="tpu_custom_call" | custom-call | tf_op jit(solution)/shard_map/pallas_call | solution.py:511
  98.1 1.2 %copy.16 = bf16[64,4,512]{2,1,0:T(4,128)(2,1)S(1)} copy(bf16[64,4,512]{2,0,1:T(8,128)(2,1)} %bitcast.9) | data formatting | bytes 524288 | tf_op jit(solution)/shard_map/transpose | solution.py:531
  99.2 0.9 reshape.3
Async XLA Ops:
  0.0 6.4 %copy-start = (bf16[32,256]{1,0:T(8,128)(2,1)S(1)}, bf16[32,256]{1,0:T(8,128)(2,1)}, u32[]{:S(2)}) copy-start(bf16[32,256]{1,0:T(8,128)(2,1)} %param.21) | copy-start | bytes 49156
  0.0 1.2 %copy-start.1 = (bf16[512,256]{1,0:T(8,128)(2,1)S(1)}, bf16[512,256]{1,0:T(8,128)(2,1)}, u32[]{:S(2)}) copy-start(bf16[512,256]{1,0:T(8,128)(2,1)} %param.18) | copy-start | bytes 786436
  0.0 1.2 %copy-start.2 = (bf16[512,256]{1,0:T(8,128)(2,1)S(1)}, bf16[512,256]{1,0:T(8,128)(2,1)}, u32[]{:S(2)}) copy-start(bf16[512,256]{1,0:T(8,128)(2,1)} %param.17) | copy-start | bytes 786436
  5.1 0.7 copy-start.4
  6.4 0.7 copy-start.3

commit v3 on v2

--- a/solution.py
+++ b/solution.py
@@ -26,18 +26,6 @@
     return values * lax.rsqrt(mean_square + EPS) * gain
 
 
-def quarter(weight, along):
-    width = weight.shape[along] // lax.axis_size("fs")
-    return lax.dynamic_slice_in_dim(weight, lax.axis_index("fs") * width, width, along)
-
-
-def shared(weight, heads):
-    group = SWA_HEADS // KV_HEADS
-    first = (lax.axis_index("fs") * heads) // group
-    count = max(1, heads // group)
-    return lax.dynamic_slice_in_dim(weight, first * HEAD_DIM, count * HEAD_DIM, 1)
-
-
 def nt(a, b):
     return lax.dot_general(a, b, (((1,), (1,)), ((), ())), preferred_element_type=F32)
 
@@ -59,9 +47,15 @@
 def mixer_kernel(
     sizes,
     tok_ref,
-    win_ref,
+    gv_ref,
+    wq_ref,
+    gq_ref,
+    gk_ref,
+    wk_ref,
+    wv_ref,
     low_ref,
-    wout_ref,
+    go_ref,
+    wo_ref,
     ngain_ref,
     up_ref,
     bias_ref,
@@ -93,6 +87,12 @@
     w_recv,
     l_send,
     l_recv,
+    v_send,
+    v_recv,
+    vp_send,
+    vp_recv,
+    lp_send,
+    lp_recv,
     o_send,
     o_recv,
     edge_sem,
@@ -111,7 +111,7 @@
     mine = f * tp + c
     own = tok_ref.shape[0]
     rows = own * tp
-    kc = win_ref.shape[0]
+    kc = gv_ref.shape[0]
     MESH = pl.DeviceIdType.MESH
 
     def remote(src, dst, ssem, rsem, target):
@@ -126,19 +126,60 @@
     def w_copy(s, way, first):
         target = {"sp": me + (1 if way == 0 else -1)}
         return remote(
-            win_ref if first else w_rows(s), w_rows(s), w_send.at[way, s], w_recv.at[s], target
+            w_main(s), w_main(s), w_send.at[way, s], w_recv.at[s], target
         )
 
-    def l_copy(s, way, first):
+    side = f % 2
+    part = kc // 2
+    lpart = low_ref.shape[0] // 2
+
+    def w_main(s):
+        return w_rows(s).at[:, : starts[4]]
+
+    def v_rows(s, h):
+        at = pl.multiple_of(s * kc + h * part, part)
+        return w_buf.at[pl.ds(at, part), starts[4] : starts[4] + 2 * HEAD_DIM]
+
+    def l_rows(s, h):
+        return l_buf.at[s, pl.ds(pl.multiple_of(h * lpart, lpart), lpart)]
+
+    def v_copy(s, way):
         target = {"sp": me + (1 if way == 0 else -1)}
-        return remote(
-            low_ref if first else l_buf.at[s], l_buf.at[s], l_send.at[way, s], l_recv.at[s], target
+        return remote(v_rows(s, side), v_rows(s, side), v_send.at[way, s], v_recv.at[s], target)
+
+    def lh_copy(s, way):
+        target = {"sp": me + (1 if way == 0 else -1)}
+        return remote(l_rows(s, side), l_rows(s, side), l_send.at[way, s], l_recv.at[s], target)
+
+    def pair_copies(s, h):
+        target = {"fs": f + 1 - 2 * side}
+        return (
+            remote(v_rows(s, h), v_rows(s, h), vp_send.at[s], vp_recv.at[s], target),
+            remote(l_rows(s, h), l_rows(s, h), lp_send.at[s], lp_recv.at[s], target),
         )
+
+    class l_copy:
+        def __init__(self, s, way, first):
+            self.s = s
+            self.both = (v_copy(s, way), lh_copy(s, way))
+
+        def start(self):
+            for copy in self.both:
+                copy.start()
+
+        def wait_recv(self):
+            for copy, onward in zip(self.both, pair_copies(self.s, side)):
+                copy.wait_recv()
+                onward.start()
+
+        def wait_send(self):
+            for copy in self.both:
+                copy.wait_send()
 
     def o_copy(s, way, first):
         target = {"sp": me + (1 if way == 0 else -1)}
         return remote(
-            wout_ref if first else o_buf.at[s], o_buf.at[s], o_send.at[way, s], o_recv.at[s], target
+            o_buf.at[s], o_buf.at[s], o_send.at[way, s], o_recv.at[s], target
         )
 
     def tok_rows(i):
@@ -150,12 +191,48 @@
             {"fs": peer // tp, "tp": peer % tp},
         )
 
+    def pick(ref, width, which):
+        value = ref[:, :width]
+        for i in range(1, ref.shape[1] // width):
+            value = jnp.where(which == i, ref[:, i * width : (i + 1) * width], value)
+        return value
+
+    def lanes(ref, width):
+        return ref.at[:, pl.ds(pl.multiple_of(f * width, width), width)]
+
+    def depth(ref, width):
+        return ref.at[pl.ds(pl.multiple_of(f * width, width), width)]
+
+    cols = [VALUE_DIM, 2 * HEAD_DIM, KEY_DIM, KEY_DIM, HEAD_DIM, HEAD_DIM]
+    starts = [sum(cols[:i]) for i in range(len(cols))]
+    gd = go_ref.shape[0] // fs
+    wd = wo_ref.shape[0] // fs
+    heads = sink_ref.shape[1] // fs
+    copies_in = [
+        (lanes(gv_ref, cols[0]), w_rows(me).at[:, : cols[0]]),
+        (lanes(wq_ref, cols[1]), w_rows(me).at[:, starts[1] : starts[2]]),
+        (depth(go_ref, gd), o_buf.at[me, pl.ds(0, gd)]),
+        (depth(wo_ref, wd), o_buf.at[me, pl.ds(gd, wd)]),
+        (low_ref, l_buf.at[me]),
+        (tok_ref, tok_rows(mine)),
+    ]
     locals_ = [
-        pltpu.make_async_copy(win_ref, w_rows(me), local_sem.at[0]),
-        pltpu.make_async_copy(low_ref, l_buf.at[me], local_sem.at[1]),
-        pltpu.make_async_copy(wout_ref, o_buf.at[me], local_sem.at[2]),
-        pltpu.make_async_copy(tok_ref, tok_rows(mine), local_sem.at[3]),
+        pltpu.make_async_copy(a, b, local_sem.at[i]) for i, (a, b) in enumerate(copies_in)
     ]
+    for copy in locals_:
+        copy.start()
+    for d in range(1, plane):
+        tok_copy(d, lax.rem(mine + d, plane), mine).start()
+    own_rows = pl.ds(pl.multiple_of(me * kc, kc), kc)
+    kv = (f * heads) // (SWA_HEADS // KV_HEADS)
+    w_buf[own_rows, starts[2] : starts[4]] = jnp.concatenate(
+        [pick(gq_ref, KEY_DIM, f), pick(gk_ref, KEY_DIM, f)], 1
+    )
+    w_buf[own_rows, starts[4] :] = jnp.concatenate(
+        [pick(wk_ref, HEAD_DIM, kv), pick(wv_ref, HEAD_DIM, kv)], 1
+    )
+    for copy in locals_[:5]:
+        copy.wait()
 
     def sends(k):
         @pl.when((me - k >= 0) & (me + 1 < sp))
@@ -178,11 +255,6 @@
 
     for k in range(sp - 1):
         sends(k)
-        if k == 0:
-            for d in range(1, plane):
-                tok_copy(d, lax.rem(mine + d, plane), mine).start()
-            for copy in locals_:
-                copy.start()
 
         @pl.when(me - 1 - k >= 0)
         def _():
@@ -206,13 +278,17 @@
             o_copy(me + k, 1, False).wait_recv()
             o_copy(me + k, 1, False).start()
 
-    for copy in locals_:
+    for copy in locals_[5:]:
         copy.wait()
+    for i in range(sp):
+        @pl.when(i != me)
+        def _():
+            for copy in pair_copies(i, 1 - side):
+                copy.wait_recv()
+
     for d in range(1, plane):
         tok_copy(d, mine, lax.rem(mine + plane - d, plane)).wait_recv()
 
-    cols = [VALUE_DIM, 2 * HEAD_DIM, KEY_DIM, KEY_DIM, HEAD_DIM, HEAD_DIM]
-    starts = [sum(cols[:i]) for i in range(len(cols))]
 
     def project(b, _):
         x = x_buf[pl.ds(pl.multiple_of(b * rows, rows), rows)].astype(F32)
@@ -244,9 +320,12 @@
         >= lax.broadcasted_iota(jnp.int32, (SPAN, SPAN), 1)
     )
     tri = lower.astype(F32)
+    up = pick(up_ref, KEY_DIM, f)
+    bias = pick(bias_ref, KEY_DIM, f)
+    sinks = pick(sink_ref, heads, f)
     for b in range(fs):
         low = proj[b, :, low_at : low_at + up_ref.shape[0]]
-        z = nn(low, up_ref[...]) + bias_ref[...]
+        z = nn(low, up) + bias
         rate = (jnp.minimum(z, 0.0) - jnp.log1p(jnp.exp(-jnp.abs(z)))) / SOFTMAX_TEMPER
         state = None
         before = jnp.zeros((1, KEY_DIM), F32)
@@ -294,7 +373,6 @@
     ki = lax.broadcasted_iota(jnp.int32, (WINDOW, 2 * WINDOW), 1)
     distance = qi + WINDOW - ki
     inside = (distance >= 0) & (distance < WINDOW)
-    heads = sink_ref.shape[1]
     for b in range(fs):
         for w in range(rows // WINDOW):
             r0 = w * WINDOW
@@ -312,7 +390,7 @@
                 q0 = starts[1] + h * HEAD_DIM
                 q = proj[b, r0 : r0 + WINDOW, q0 : q0 + HEAD_DIM]
                 s = jnp.where(valid, nt(q, bk) * HEAD_DIM**-0.5, -1e30)
-                sink = sink_ref[0:1, h : h + 1]
+                sink = sinks[:, h : h + 1]
                 top = jnp.maximum(jnp.max(s, -1, keepdims=True), sink)
                 e = jnp.exp(s - top)
                 den = jnp.sum(e, -1, keepdims=True) + jnp.exp(sink - top)
@@ -418,6 +496,12 @@
             l_copy(me + k, 1, False).wait_send()
             w_copy(me + k, 1, False).wait_send()
             o_copy(me + k, 1, False).wait_send()
+
+    for i in range(sp):
+        @pl.when(i != me)
+        def _():
+            for copy in pair_copies(i, side):
+                copy.wait_send()
 
     for d in range(1, plane):
         tok_copy(d, mine, mine).wait_send()
@@ -450,25 +534,14 @@
     window_output_weight,
 ):
     fs, tp, sp = (lax.axis_size(n) for n in ("fs", "tp", "sp"))
-    heads = sink_logit.shape[0] // fs
-    w_in = jnp.concatenate(
-        [
-            quarter(gla_value_weight, 1),
-            quarter(window_query_weight, 1),
-            quarter(gla_query_weight, 1),
-            quarter(gla_key_weight, 1),
-            shared(window_key_weight, heads),
-            shared(window_value_weight, heads),
-        ],
-        1,
-    )
     low = decay_down.T
-    w_out = jnp.concatenate([quarter(gla_output_weight, 0), quarter(window_output_weight, 0)], 0)
     own = tokens.shape[1]
     rows = own * tp
-    kc, width = w_in.shape
+    kc = decay_down.shape[0]
+    width = VALUE_DIM + 4 * HEAD_DIM + 2 * KEY_DIM
     rank = low.shape[0]
-    depth, nc = w_out.shape
+    depth = (gla_output_weight.shape[0] + window_output_weight.shape[0]) // fs
+    nc = gla_output_weight.shape[1]
     vm = pltpu.VMEM
     dma = pltpu.SemaphoreType.DMA
     scratch = [
@@ -490,12 +563,18 @@
         vm((sp, fs - 1, own, nc), BF),
         vm((sp, fs - 1, own, nc), BF),
         vm((sp, own, nc), F32),
-        dma((4,)),
+        dma((6,)),
         dma((fs * tp - 1,)),
         dma((fs * tp - 1,)),
         dma((2, sp)),
         dma((sp,)),
         dma((2, sp)),
+        dma((sp,)),
+        dma((2, sp)),
+        dma((sp,)),
+        dma((sp,)),
+        dma((sp,)),
+        dma((sp,)),
         dma((sp,)),
         dma((2, sp)),
         dma((sp,)),
@@ -508,10 +587,13 @@
         dma((sp, fs - 1)),
     ]
     spec = pl.BlockSpec(memory_space=pltpu.VMEM)
+    anywhere = pl.BlockSpec(memory_space=pl.ANY)
     mixed = pl.pallas_call(
         functools.partial(mixer_kernel, (sp, fs, tp)),
         out_shape=jax.ShapeDtypeStruct((sp, own, nc), BF),
-        in_specs=[spec] * 9,
+        in_specs=[
+            anywhere if i in (1, 2, 8, 9) else spec for i in range(15)
+        ],
         out_specs=spec,
         scratch_shapes=scratch,
         compiler_params=pltpu.CompilerParams(
@@ -519,14 +601,20 @@
         ),
     )(
         tokens[0],
-        w_in,
+        gla_value_weight,
+        window_query_weight,
+        gla_query_weight,
+        gla_key_weight,
+        window_key_weight,
+        window_value_weight,
         low,
-        w_out,
+        gla_output_weight,
+        window_output_weight,
         norm_gain[None],
-        quarter(decay_up, 1),
-        quarter(decay_bias, 0)[None],
+        decay_up,
+        decay_bias[None],
         head_gain[None],
-        quarter(sink_logit, 0)[None],
+        sink_logit[None],
     )
     return mixed.transpose(1, 0, 2).reshape(1, own, sp * nc)
 

time: 100 us -> 88.7 us (0.89)
  local copies, waits for them, and re-layouts: 8.99 us -> 2.04 us
  Pallas kernels: 90.3 us -> 86.5 us
    dynamic_slice x5 -> x0, local copies, waits for them, and re-layouts: 3.96 us -> none  [the longest x4 2.79 us: quarter(): lax.dynamic_slice_in_dim(weight, lax.axis_index('fs') * width, width, along)]
    pallas_call x1, Pallas kernels: 90.3 us -> 86.5 us  [per_device(): pl.pallas_call(functools.partial(mixer_kernel, (sp, fs, tp)), out_shape=j...]
    broadcast_in_dim x2 -> x0, local copies, waits for them, and re-layouts: 1.25 us -> none  [the longest x1 0.64 us: per_device(): quarter(decay_bias, 0)[None]]
    concatenate x1 -> x0, local copies, waits for them, and re-layouts: 1.07 us -> none  [per_device(): jnp.concatenate([quarter(gla_value_weight, 1), quarter(window_query_weigh...]
where the time goes in v3:
time: 88.7 us; the launch traced here: 88.5 us
  Pallas kernels  86.5 us (98%)
  local copies, waits for them, and re-layouts  2.04 us (2%)
    pallas_call x1, Pallas kernels, per_device(): pl.pallas_call(functools.partial(mixer_kernel, (sp, fs, tp)), out_shape=j...  86.5 us

profile of v3, /device:TPU:25, one launch (start us, length us, event | category | flops | bytes accessed | tf_op | source)
XLA Modules:
  0.0 88.5 jit_solution(2615315040558513929)
XLA Ops:
  0.0 86.5 %shard_map.145 = bf16[4,64,512]{2,1,0:T(8,128)(2,1)} custom-call(bf16[64,2048]{1,0:T(8,128)(2,1)} %bitcast.8, bf16[512,512]{1,0:T(8,128)(2,1)} %gv_ref.1, bf16[512,512]{1,0:T(8,128)(2,1)} %wq_ref.1, bf16[512,256]{1,0:T(8,128)(2,1)} %gq_ref.1, bf16[512,256]{1,0:T(8,128)(2,1)} %gk_ref.1, bf16[512,128]{1,0:T(8,128)(2,1)} %wk_ref.1, bf16[512,128]{1,0:T(8,128)(2,1)} %wv_ref.1, ...), custom_call_target="tpu_custom_call" | custom-call | tf_op jit(solution)/shard_map/pallas_call | solution.py:591
  86.5 1.2 %copy.16 = bf16[64,4,512]{2,1,0:T(4,128)(2,1)S(1)} copy(bf16[64,4,512]{2,0,1:T(8,128)(2,1)} %bitcast.7) | data formatting | bytes 524288 | tf_op jit(solution)/shard_map/transpose | solution.py:619
  87.7 0.9 reshape.3

commit v4 on v3

--- a/solution.py
+++ b/solution.py
@@ -462,7 +462,10 @@
         for d in range(1, fs):
             piece_copy(s, d, f).wait_recv()
             total += piece_in[s, d - 1].astype(F32)
-        out_ref[s] = total.astype(BF)
+        if len(out_ref.shape) == 2:
+            out_ref[:, pl.ds(pl.multiple_of(s * nc, nc), nc)] = total.astype(BF)
+        else:
+            out_ref[s] = total.astype(BF)
 
     produce(0)
 
@@ -542,6 +545,7 @@
     rank = low.shape[0]
     depth = (gla_output_weight.shape[0] + window_output_weight.shape[0]) // fs
     nc = gla_output_weight.shape[1]
+    flat = nc % 128 == 0
     vm = pltpu.VMEM
     dma = pltpu.SemaphoreType.DMA
     scratch = [
@@ -590,7 +594,7 @@
     anywhere = pl.BlockSpec(memory_space=pl.ANY)
     mixed = pl.pallas_call(
         functools.partial(mixer_kernel, (sp, fs, tp)),
-        out_shape=jax.ShapeDtypeStruct((sp, own, nc), BF),
+        out_shape=jax.ShapeDtypeStruct((own, sp * nc) if flat else (sp, own, nc), BF),
         in_specs=[
             anywhere if i in (1, 2, 8, 9) else spec for i in range(15)
         ],
@@ -616,7 +620,7 @@
         head_gain[None],
         sink_logit[None],
     )
-    return mixed.transpose(1, 0, 2).reshape(1, own, sp * nc)
+    return (mixed if flat else mixed.transpose(1, 0, 2)).reshape(1, own, sp * nc)
 
 
 def solution(mesh):

time: 88.7 us -> 88.4 us (level)
    unnamed x0 -> x1, local copies, waits for them, and re-layouts: none -> 1.67 us
    transpose x1 -> x0, local copies, waits for them, and re-layouts: 1.16 us -> none  [per_device(): return mixed.transpose(1, 0, 2).reshape(1, own, sp * nc)]
where the time goes in v4:
time: 88.4 us; the launch traced here: 88.2 us
  Pallas kernels  86.5 us (98%)
  local copies, waits for them, and re-layouts  1.67 us (2%)
    pallas_call x1, Pallas kernels, per_device(): pl.pallas_call(functools.partial(mixer_kernel, (sp, fs, tp)), out_shape=j...  86.5 us

profile of v4, /device:TPU:25, one launch (start us, length us, event | category | flops | bytes accessed | tf_op | source)
XLA Modules:
  0.0 88.2 jit_solution(6236679166635708858)
XLA Ops:
  0.0 86.5 %shard_map.145 = bf16[64,2048]{1,0:T(8,128)(2,1)} custom-call(bf16[64,2048]{1,0:T(8,128)(2,1)} %bitcast.8, bf16[512,512]{1,0:T(8,128)(2,1)} %gv_ref.1, bf16[512,512]{1,0:T(8,128)(2,1)} %wq_ref.1, bf16[512,256]{1,0:T(8,128)(2,1)} %gq_ref.1, bf16[512,256]{1,0:T(8,128)(2,1)} %gk_ref.1, bf16[512,128]{1,0:T(8,128)(2,1)} %wk_ref.1, bf16[512,128]{1,0:T(8,128)(2,1)} %wv_ref.1, ...), custom_call_target="tpu_custom_call" | custom-call | tf_op jit(solution)/shard_map/pallas_call | solution.py:595
  86.5 1.7 %copy.17 = bf16[1,64,2048]{2,1,0:T(8,128)(2,1)} copy(bf16[1,64,2048]{2,1,0:T(8,128)(2,1)} %bitcast.7) | data formatting | bytes 524288
